TPU v7x, 512 devices: a 8x2x16 block of a 8x16x16 slice. The times are simulated.
512 devices in a mesh: grp: 2 (over y), fs: 16 (over z), tp: 16 (over x, core).
Axes of the slice: x: 8, y: 2, z: 16, core: 2. Of those that a mesh axis runs over, the one named last changes fastest.
The devices are a block of a 8x16x16 slice.
Arguments:
- tokens: bfloat16 [4096, 2048], P(('grp', 'fs')), parts along dimension 0, may hold values from -12 to 12, as said below
- mix_heads: bfloat16 [4096, 2048], P(('grp', 'fs'), 'tp'), parts along dimension 0, may hold values from -6 to 6
- norm_first: float32 [2048], replicated, may hold values from 0.1 to 1.9
- gate_first: bfloat16 [2048, 5632], P('fs', 'tp'), may hold values from -0.125 to 0.125
- up_first: bfloat16 [2048, 5632], P('fs', 'tp'), may hold values from -0.125 to 0.125
- down_first: bfloat16 [5632, 2048], P('tp', 'fs'), may hold values from -0.078125 to 0.078125
- out_weight: bfloat16 [2048, 2048], P('tp', 'fs'), may hold values from -0.125 to 0.125
- norm_second: float32 [2048], replicated, may hold values from 0.1 to 1.9
- gate_second: bfloat16 [2048, 5632], P('fs', 'tp'), may hold values from -0.125 to 0.125
- up_second: bfloat16 [2048, 5632], P('fs', 'tp'), may hold values from -0.125 to 0.125
- down_second: bfloat16 [5632, 2048], P('tp', 'fs'), may hold values from -0.078125 to 0.078125
Outputs:
- layer_out: bfloat16 [4096, 2048], P(('grp', 'fs')), parts along dimension 0
There are 2 independent parts, one for each index of `grp`. A program takes and returns all parts, laid end to end along the dimension named above; an argument that names none is the same for every part. Nothing has to cross between parts.
Inputs may be any that keep to these rules, and one draw needn't show every extreme that they name: Each row of tokens carries a scale of its own.
All inputs are finite; a program needn't handle non-finite values.
Results may differ from a plain program's by a relative error of at most 0.014.
Values may be sent and summed in bfloat16 or wider, within the bound.
A program may use at most 64 MiB of HBM per device.

v0:
```python
import jax
import jax.numpy as jnp
from jax import lax
from jax.sharding import PartitionSpec as P

EPS = 0.1


def side_by_side(arrays, axis, dim, along):
    both = jnp.concatenate(arrays, axis=along)
    result, at, done = (lax.all_gather(both, axis, axis=dim, tiled=True), 0, [])
    for a in arrays:
        done.append(lax.slice_in_dim(result, at, at + a.shape[along], axis=along))
        at += a.shape[along]
    return tuple(done)


def laid_out(tiles, dim):
    lengths = list(tiles.shape[1:])
    lengths[dim] *= tiles.shape[0]
    return jnp.moveaxis(tiles, 0, dim).reshape(lengths)


def sent_to_all(array, axis):
    size = lax.axis_size(axis)
    return lax.all_to_all(
        jnp.broadcast_to(array[None], (size, *array.shape)), axis, 0, 0, tiled=True
    )


def gather_directly(array, axis, dim):
    return laid_out(sent_to_all(array, axis), dim)


def in_blocks(array, dim, size):
    before, after = (array.shape[:dim], array.shape[dim + 1 :])
    return jnp.moveaxis(array.reshape(*before, size, -1, *after), dim, 0)


def sum_at_owner(array, axis, dim):
    size = lax.axis_size(axis)
    tiles = lax.all_to_all(in_blocks(array, dim, size), axis, 0, 0, tiled=True)
    return jnp.sum(tiles.astype(jnp.float32), axis=0)


def norm_rows(row_block, gain_vector):
    widened = row_block.astype(jnp.float32)
    scaled = widened * lax.rsqrt(jnp.mean(widened * widened, axis=-1, keepdims=True) + EPS)
    return (scaled * gain_vector).astype(jnp.bfloat16)


def gate_values(normed, gate_weight, value_weight):
    pieces = side_by_side((gate_weight, value_weight), "fs", 0, 1)
    return (
        jnp.dot(normed, pieces[0], preferred_element_type=jnp.float32),
        jnp.dot(normed, pieces[1], preferred_element_type=jnp.float32),
    )


def half_branch(normed, gate_weight, value_weight, down_weight):
    gates, values = gate_values(normed, gate_weight, value_weight)
    hidden = (jax.nn.silu(gates) * values).astype(jnp.bfloat16)
    return 0.5 * jnp.dot(
        hidden, gather_directly(down_weight, "fs", 1), preferred_element_type=jnp.float32
    )


def share_sum(block_terms):
    return sum_at_owner(block_terms.astype(jnp.bfloat16), "tp", 0)


def join_rows(row_block):
    return lax.all_gather(row_block, "tp", axis=0, tiled=True)


def local(
    tokens,
    mix_heads,
    norm_first,
    gate_first,
    up_first,
    down_first,
    out_weight,
    norm_second,
    gate_second,
    up_second,
    down_second,
):
    normed_one = norm_rows(tokens, norm_first)
    first_terms = half_branch(normed_one, gate_first, up_first, down_first)
    heads_out = jnp.dot(
        mix_heads, gather_directly(out_weight, "fs", 1), preferred_element_type=jnp.float32
    )
    first_terms = first_terms + heads_out
    share_rows = tokens.shape[0] // lax.axis_size("tp")
    offset = lax.axis_index("tp") * share_rows
    own_rows = lax.dynamic_slice_in_dim(tokens, offset, share_rows, 0).astype(jnp.float32)
    resid_two = own_rows + share_sum(first_terms)
    normed_two = join_rows(norm_rows(resid_two, norm_second))
    second_terms = half_branch(normed_two, gate_second, up_second, down_second)
    finished = (resid_two + share_sum(second_terms)).astype(jnp.bfloat16)
    return join_rows(finished)


def solution(mesh):
    in_specs = (
        P(("grp", "fs"), None),
        P(("grp", "fs"), "tp"),
        P(),
        P("fs", "tp"),
        P("fs", "tp"),
        P("tp", "fs"),
        P("tp", "fs"),
        P(),
        P("fs", "tp"),
        P("fs", "tp"),
        P("tp", "fs"),
    )
    out_specs = P(("grp", "fs"), None)
    return jax.shard_map(local, mesh=mesh, in_specs=in_specs, out_specs=out_specs, check_vma=False)
```

profile of v0, /device:TPU:65, one launch (start us, length us, event | category | flops | bytes accessed | tf_op | source)
XLA Modules:
  0.0 398.9 jit_solution(9208464378308235055)
XLA Ops:
  6.6 2.2 broadcast_in_dim.6
  8.8 44.4 %all-to-all-start = ((bf16[16,352,128]{2,1,0:T(8,128)(2,1)}), bf16[16,352,128]{2,1,0:T(8,128)(2,1)S(1)}, u32[]{:S(2)}, u32[]{:S(2)}) async-start(bf16[16,352,128]{2,1,0:T(8,128)(2,1)} %broadcast_in_dim.6), calls=%async_computation | async-start | bytes 2883584 | tf_op jit(solution)/shard_map/all_to_all | solution.py:26
  53.1 0.1 all-gather.3.cloned.1.call-start
  53.2 0.7 pad_maximum_fusion
  53.9 0.1 all-gather.3.cloned.1.call-update
  54.0 0.1 copy.14
  54.1 68.0 %all-to-all-done = bf16[16,352,128]{2,1,0:T(8,128)(2,1)S(1)} async-done(((bf16[16,352,128]{2,1,0:T(8,128)(2,1)}), bf16[16,352,128]{2,1,0:T(8,128)(2,1)S(1)}, u32[]{:S(2)}, u32[]{:S(2)}) %all-to-all-start) | async-done | bytes 1441824 | tf_op jit(solution)/shard_map/all_to_all | solution.py:26
  122.1 0.9 broadcast_in_dim.7
  123.0 13.5 %all-to-all-start.1 = ((bf16[16,128,128]{1,2,0:T(8,128)(2,1)}), bf16[16,128,128]{1,2,0:T(8,128)(2,1)S(1)}, u32[]{:S(2)}, u32[]{:S(2)}) async-start(bf16[16,128,128]{1,2,0:T(8,128)(2,1)} %broadcast_in_dim.7), calls=%async_computation.1 | async-start | bytes 1048576 | tf_op jit(solution)/shard_map/all_to_all | solution.py:26
  136.6 0.2 fusion.30
  136.8 48.7 %all-gather.3.cloned.1.call-done = bf16[2048,704]{0,1:T(8,128)(2,1)} async-done(((bf16[128,704]{0,1:T(8,128)(2,1)}), bf16[2048,704]{0,1:T(8,128)(2,1)}) %all-gather.3.cloned.1.call-update) | async-done | bytes 2883600 | tf_op jit(solution)/shard_map/all_gather | solution.py:11
  185.5 2.0 fusion.14
  187.5 3.1 convolution_multiply_fusion.1
  190.6 1.1 fusion.3
  191.7 15.7 %all-to-all-start.2 = ((bf16[16,8,2048]{2,1,0:T(8,128)(2,1)}), bf16[16,8,2048]{2,1,0:T(8,128)(2,1)S(1)}, u32[]{:S(2)}, u32[]{:S(2)}) async-start(bf16[16,8,2048]{2,1,0:T(8,128)(2,1)} %fusion.3), calls=%async_computation.2 | async-start | bytes 1048576 | tf_op jit(solution)/shard_map/all_to_all | solution.py:42
  207.4 0.1 all-gather.5.cloned.1.call-start
  207.5 0.7 pad_maximum_fusion.1
  208.3 16.4 %all-to-all-done.2 = bf16[16,8,2048]{2,1,0:T(8,128)(2,1)S(1)} async-done(((bf16[16,8,2048]{2,1,0:T(8,128)(2,1)}), bf16[16,8,2048]{2,1,0:T(8,128)(2,1)S(1)}, u32[]{:S(2)}, u32[]{:S(2)}) %all-to-all-start.2) | async-done | bytes 524320 | tf_op jit(solution)/shard_map/all_to_all | solution.py:42
  224.6 1.3 broadcast_in_dim.8
  225.9 8.3 %all-to-all-start.3 = ((bf16[16,352,128]{2,1,0:T(8,128)(2,1)}), bf16[16,352,128]{2,1,0:T(8,128)(2,1)S(1)}, u32[]{:S(2)}, u32[]{:S(2)}) async-start(bf16[16,352,128]{2,1,0:T(8,128)(2,1)} %broadcast_in_dim.8), calls=%async_computation.3 | async-start | bytes 2883584 | tf_op jit(solution)/shard_map/all_to_all | solution.py:26
  234.2 0.1 convert_reduce_fusion.1
  234.3 0.9 multiply_reduce_fusion
  235.2 0.8 multiply_convert_fusion
  236.0 16.0 %all_gather.13 = bf16[128,2048]{1,0:T(8,128)(2,1)S(1)} all-gather(bf16[8,2048]{1,0:T(8,128)(2,1)S(1)} %multiply_convert_fusion), channel_id=1, replica_groups=mesh['grp'=2,'fs'=16,'tp'=16] {'tp'}, dimensions={0}, use_global_device_ids=true | all-gather | bytes 557056 | tf_op jit(solution)/shard_map/all_gather | solution.py:73
  252.0 86.3 %all-gather.5.cloned.1.call-done = bf16[2048,704]{0,1:T(8,128)(2,1)} async-done(((bf16[128,704]{0,1:T(8,128)(2,1)}), bf16[2048,704]{0,1:T(8,128)(2,1)}) %all-gather.5.cloned.1.call-update) | async-done | bytes 2883600 | tf_op jit(solution)/shard_map/all_gather | solution.py:11
  338.3 1.9 fusion.10
  340.2 2.8 fusion.2
  343.1 31.3 %all_to_all.25 = bf16[16,8,2048]{2,1,0:T(8,128)(2,1)S(1)} all-to-all(bf16[16,8,2048]{2,1,0:T(8,128)(2,1)S(1)} %fusion.2), channel_id=1, replica_groups=mesh['grp'=2,'fs'=16,'tp'=16] {'tp'}, dimensions={0} | all-to-all | bytes 1048576 | tf_op jit(solution)/shard_map/all_to_all | solution.py:42
  374.4 0.1 convert_reduce_fusion
  374.5 0.8 add_convert_fusion
  375.2 16.0 %all_gather.15 = bf16[128,2048]{1,0:T(8,128)(2,1)S(1)} all-gather(bf16[8,2048]{1,0:T(8,128)(2,1)S(1)} %add_convert_fusion), channel_id=1, replica_groups=mesh['grp'=2,'fs'=16,'tp'=16] {'tp'}, dimensions={0}, use_global_device_ids=true | all-gather | bytes 557056 | tf_op jit(solution)/shard_map/all_gather | solution.py:73
  391.2 0.8 copy.27
  (25 shorter events, 0.1 us)
Async XLA Ops:
  6.5 184.0 %copy-start = (bf16[128,128]{1,0:T(8,128)(2,1)S(1)}, bf16[128,128]{1,0:T(8,128)(2,1)}, u32[]{:S(2)}) copy-start(bf16[128,128]{1,0:T(8,128)(2,1)} %param.12) | copy-start | bytes 98308
  8.8 44.5 %copy-start.2 = (bf16[128,352]{0,1:T(8,128)(2,1)S(1)}, bf16[128,352]{0,1:T(8,128)(2,1)}, u32[]{:S(2)}) copy-start(bf16[128,352]{0,1:T(8,128)(2,1)} %param.15) | copy-start | bytes 270340
  8.8 44.5 %copy-start.3 = (bf16[128,352]{0,1:T(8,128)(2,1)S(1)}, bf16[128,352]{0,1:T(8,128)(2,1)}, u32[]{:S(2)}) copy-start(bf16[128,352]{0,1:T(8,128)(2,1)} %param.14) | copy-start | bytes 270340
  8.8 45.2 %copy-start.7 = (bf16[128,128]{1,0:T(8,128)(2,1)S(1)}, bf16[128,128]{1,0:T(8,128)(2,1)}, u32[]{:S(2)}) copy-start(bf16[128,128]{1,0:T(8,128)(2,1)} %param.17) | copy-start | bytes 98308
  8.8 113.4 %all-to-all-start = ((bf16[16,352,128]{2,1,0:T(8,128)(2,1)}), bf16[16,352,128]{2,1,0:T(8,128)(2,1)S(1)}, u32[]{:S(2)}, u32[]{:S(2)}) async-start(bf16[16,352,128]{2,1,0:T(8,128)(2,1)} %broadcast_in_dim.6), calls=%async_computation | async-start | bytes 2883584 | tf_op jit(solution)/shard_map/all_to_all | solution.py:26
  53.1 83.4 %copy-start.1 = (bf16[128,2048]{1,0:T(8,128)(2,1)S(1)}, bf16[128,2048]{1,0:T(8,128)(2,1)}, u32[]{:S(2)}) copy-start(bf16[128,2048]{1,0:T(8,128)(2,1)} %param.11) | copy-start | bytes 1572868
  53.1 132.4 %copy-start.9 = (f32[2048]{0:T(1024)S(1)}, f32[2048]{0:T(1024)}, u32[]{:S(2)}) copy-start(f32[2048]{0:T(1024)} %param.13) | copy-start | bytes 24580
  53.1 132.3 %all-gather.3.cloned.1.call-start = ((), (), s32[]{:S(2)}) async-start(), calls=%async_computation.5 | async-start | bytes 3063808 | tf_op jit(solution)/shard_map/all_gather | solution.py:11
  123.0 67.6 %all-to-all-start.1 = ((bf16[16,128,128]{1,2,0:T(8,128)(2,1)}), bf16[16,128,128]{1,2,0:T(8,128)(2,1)S(1)}, u32[]{:S(2)}, u32[]{:S(2)}) async-start(bf16[16,128,128]{1,2,0:T(8,128)(2,1)} %broadcast_in_dim.7), calls=%async_computation.1 | async-start | bytes 1048576 | tf_op jit(solution)/shard_map/all_to_all | solution.py:26
  190.6 16.9 %copy-start.4 = (bf16[128,352]{0,1:T(8,128)(2,1)S(1)}, bf16[128,352]{0,1:T(8,128)(2,1)}, u32[]{:S(2)}) copy-start(bf16[128,352]{0,1:T(8,128)(2,1)} %param.20) | copy-start | bytes 270340
  190.6 16.9 %copy-start.5 = (bf16[128,352]{0,1:T(8,128)(2,1)S(1)}, bf16[128,352]{0,1:T(8,128)(2,1)}, u32[]{:S(2)}) copy-start(bf16[128,352]{0,1:T(8,128)(2,1)} %param.19) | copy-start | bytes 270340
  190.6 34.0 %copy-start.6 = (bf16[352,128]{1,0:T(8,128)(2,1)S(1)}, bf16[352,128]{1,0:T(8,128)(2,1)}, u32[]{:S(2)}) copy-start(bf16[352,128]{1,0:T(8,128)(2,1)} %param.21) | copy-start | bytes 270340
  191.7 32.9 %all-to-all-start.2 = ((bf16[16,8,2048]{2,1,0:T(8,128)(2,1)}), bf16[16,8,2048]{2,1,0:T(8,128)(2,1)S(1)}, u32[]{:S(2)}, u32[]{:S(2)}) async-start(bf16[16,8,2048]{2,1,0:T(8,128)(2,1)} %fusion.3), calls=%async_computation.2 | async-start | bytes 1048576 | tf_op jit(solution)/shard_map/all_to_all | solution.py:42
  207.4 130.9 %all-gather.5.cloned.1.call-start = ((), (), s32[]{:S(2)}) async-start(), calls=%async_computation.6 | async-start | bytes 3063808 | tf_op jit(solution)/shard_map/all_gather | solution.py:11
  225.9 9.3 %copy-start.8 = (f32[2048]{0:T(1024)S(1)}, f32[2048]{0:T(1024)}, u32[]{:S(2)}) copy-start(f32[2048]{0:T(1024)} %param.18) | copy-start | bytes 24580
  225.9 114.3 %all-to-all-start.3 = ((bf16[16,352,128]{2,1,0:T(8,128)(2,1)}), bf16[16,352,128]{2,1,0:T(8,128)(2,1)S(1)}, u32[]{:S(2)}, u32[]{:S(2)}) async-start(bf16[16,352,128]{2,1,0:T(8,128)(2,1)} %broadcast_in_dim.8), calls=%async_computation.3 | async-start | bytes 2883584 | tf_op jit(solution)/shard_map/all_to_all | solution.py:26
Sparse Core Ops, SparseCore 0:
  56.0 129.4 all-gather.2
  210.3 127.9 all-gather.4
where the time goes:
time: 400 us; the launch traced here: 399 us
  waiting for transfers between devices  220 us (55%)
  starting transfers between devices  82 us (20%)
  blocking collectives  63.3 us (16%)
  between operations  13.6 us (3%)
  matrix products  10.9 us (3%)
  local copies, waits for them, and re-layouts  5.35 us (1%)
  other arithmetic  4.25 us (1%)
    all_gather x2, waiting for transfers between devices, side_by_side(): result, at, done = (lax.all_gather(both, axis, axis=dim, tiled=True), 0, [])  135 us
    all_to_all x3, waiting for transfers between devices, sent_to_all(): lax.all_to_all(jnp.broadcast_to(array[None], (size, *array.shape)), axis,...  68 us
    all_to_all x3, starting transfers between devices, sent_to_all(): lax.all_to_all(jnp.broadcast_to(array[None], (size, *array.shape)), axis,...  66.1 us
    all_gather x2, blocking collectives, join_rows(): return lax.all_gather(row_block, 'tp', axis=0, tiled=True)  32 us
    all_to_all x1, blocking collectives, sum_at_owner(): tiles = lax.all_to_all(in_blocks(array, dim, size), axis, 0, 0, tiled=True)  31.3 us
    all_to_all x1, waiting for transfers between devices, sum_at_owner(): tiles = lax.all_to_all(in_blocks(array, dim, size), axis, 0, 0, tiled=True)  16.4 us
    all_to_all x1, starting transfers between devices, sum_at_owner(): tiles = lax.all_to_all(in_blocks(array, dim, size), axis, 0, 0, tiled=True)  15.7 us
  transfers between devices with their start and end apart: 6, of which 4 were waited for; matrix products, arithmetic and copies ran while one was open for 3% of the time, Pallas kernels for 0%

commit v1 on v0

v1 whole, which is shorter than its diff:
```python
import functools

import jax
import jax.numpy as jnp
from jax import lax
from jax.experimental import pallas as pl
from jax.experimental.pallas import tpu as pltpu
from jax.sharding import PartitionSpec as P

EPS = 0.1
PAIRED = False
RIGHT, LEFT = 0, 1
FIRST, SECOND = (0, 1, 2), (3, 4, 5)
OFFSETS = (0, 0, 1, 8, 8, 10)
SLOTS = 19
SUM_AFTER = 3
JOIN_AFTER = 3
GROUPS = ((0, 9), (9, 13), (13, 16))


def steps_positions(step):
    if step == 0:
        return (0,)
    return (15,) if step == 8 else (2 * step - 1, 2 * step)


def nt(a, b):
    return lax.dot_general(a, b, (((1,), (1,)), ((), ())), preferred_element_type=jnp.float32)


def body(
    tok, mix, gain1, gain2, g1, u1, d1, ow, g2, u2, d2,
    out,
    w0, w1, w2, w3, w4, w5, xf, x1, acc, hid, t1, r1, t2, r2, nrm, x2, fin, done, resid,
    wsem, ssem, rsem, ysend, yrecv, xsend, xrecv,
):
    W = (w0, w1, w2, w3, w4, w5)
    z, tp, gr = lax.axis_index("fs"), lax.axis_index("tp"), lax.axis_index("grp")
    nz, ntp = lax.axis_size("fs"), lax.axis_size("tp")
    right, left = lax.rem(z + 1, nz), lax.rem(z + nz - 1, nz)
    parity = lax.rem(gr, 2)
    mate = gr + 1 - 2 * parity
    share = tok.shape[0] // ntp
    wide = tok.shape[1] // nz
    hidden_rows = g1.shape[1]

    def block_of(pos):
        if pos == 0:
            return z
        if pos == 15:
            return lax.rem(z + 8, nz)
        step = (pos + 1) // 2
        return lax.rem(z + nz - step, nz) if pos % 2 else lax.rem(z + step, nz)

    def cut(c):
        rows = W[c].shape[1]
        lent = rows // 3 // 16 * 16
        if not PAIRED:
            return 0, rows, 0, 0
        return pl.multiple_of(parity * lent, 16), rows - lent, pl.multiple_of((1 - parity) * (rows - lent), 16), lent

    barrier = pltpu.get_barrier_semaphore()
    pl.semaphore_signal(barrier, device_id={"fs": right}, device_id_type=pl.DeviceIdType.MESH)
    pl.semaphore_signal(barrier, device_id={"fs": left}, device_id_type=pl.DeviceIdType.MESH)
    for d in range(1, 16):
        pl.semaphore_signal(barrier, device_id={"tp": lax.rem(tp + d, ntp)}, device_id_type=pl.DeviceIdType.MESH)
    if PAIRED:
        pl.semaphore_signal(barrier, device_id={"grp": mate}, device_id_type=pl.DeviceIdType.MESH)

    loads = [
        pltpu.make_async_copy(d1, w2.at[0, 0:hidden_rows], wsem.at[0]),
        pltpu.make_async_copy(ow, w2.at[0, hidden_rows : w2.shape[1]], wsem.at[1]),
        pltpu.make_async_copy(d2, w5.at[0], wsem.at[2]),
    ]
    for load in loads:
        load.start()
    w0[0] = g1[...].T
    w1[0] = u1[...].T
    w3[0] = g2[...].T
    w4[0] = u2[...].T
    for load in loads:
        load.wait()
    pl.semaphore_wait(barrier, 18 if PAIRED else 17)

    sends = []

    def ring_copy(c, way, step):
        start, keep, _, _ = cut(c)
        if step == 7:
            half = keep // 32 * 16
            src = 13 if way == RIGHT else 14
            dst = 15
            rows = pl.ds(start, half) if way == RIGHT else pl.ds(start + half, keep - half)
        else:
            src = 0 if step == 0 else (2 * step - 1 if way == RIGHT else 2 * step)
            dst = 2 * step + 1 if way == RIGHT else 2 * step + 2
            rows = pl.ds(start, keep)
        return pltpu.make_async_remote_copy(
            src_ref=W[c].at[src, rows], dst_ref=W[c].at[dst, rows],
            send_sem=ssem.at[c, way, step], recv_sem=rsem.at[c, way, step],
            device_id={"fs": right if way == RIGHT else left}, device_id_type=pl.DeviceIdType.MESH,
        )

    def lend_copy(c, pos):
        _, _, start, lent = cut(c)
        start = pl.multiple_of((W[c].shape[1] - lent) - start, 16)
        return pltpu.make_async_remote_copy(
            src_ref=W[c].at[pos, pl.ds(start, lent)], dst_ref=W[c].at[pos, pl.ds(start, lent)],
            send_sem=ysend.at[c, pos], recv_sem=yrecv.at[c, pos],
            device_id={"grp": mate}, device_id_type=pl.DeviceIdType.MESH,
        )

    def hop(c, step):
        if step > 0:
            ring_copy(c, RIGHT, step - 1).wait_recv()
            ring_copy(c, LEFT, step - 1).wait_recv()
        if step < 8:
            for way in (RIGHT, LEFT):
                copy = ring_copy(c, way, step)
                copy.start()
                sends.append(copy)
        if PAIRED and step > 0:
            for pos in steps_positions(step):
                copy = lend_copy(c, pos)
                copy.start()
                sends.append(copy)

    def arrived(c, step):
        if PAIRED and step > 0:
            for pos in steps_positions(step):
                _, _, start, lent = cut(c)
                rows = pl.ds(start, lent)
                pltpu.make_async_remote_copy(
                    src_ref=W[c].at[pos, rows], dst_ref=W[c].at[pos, rows],
                    send_sem=ysend.at[c, pos], recv_sem=yrecv.at[c, pos],
                    device_id={"grp": mate}, device_id_type=pl.DeviceIdType.MESH,
                ).wait_recv()

    def spread(kind, src_of, dst, lo, hi):
        for d in range(1, 16):
            peer = lax.rem(tp + d, ntp)
            copy = pltpu.make_async_remote_copy(
                src_ref=src_of(peer), dst_ref=dst.at[tp, lo:hi],
                send_sem=xsend.at[kind, d], recv_sem=xrecv.at[kind, d],
                device_id={"tp": peer}, device_id_type=pl.DeviceIdType.MESH,
            )
            copy.start()
            sends.append(copy)

    def collect(kind, dst, lo, hi):
        for d in range(1, 16):
            peer = lax.rem(tp + ntp - d, ntp)
            part = dst.at[peer, lo:hi]
            pltpu.make_async_remote_copy(
                src_ref=part, dst_ref=part, send_sem=xsend.at[kind, d], recv_sem=xrecv.at[kind, d],
                device_id={"tp": peer}, device_id_type=pl.DeviceIdType.MESH,
            ).wait_recv()

    def sum_terms(t, r, lo, hi):
        total = t[tp, lo:hi].astype(jnp.float32)
        for d in range(1, 16):
            total = total + r[lax.rem(tp + d, ntp), lo:hi].astype(jnp.float32)
        return total

    def norm_first():
        squares = jnp.zeros((tok.shape[0], wide), jnp.float32)
        for pos in range(16):
            b = block_of(pos)
            v = tok[:, pl.ds(pl.multiple_of(b * wide, wide), wide)].astype(jnp.float32)
            xf[pos] = v
            squares = squares + v * v
        scale = lax.rsqrt(jnp.sum(squares, axis=1, keepdims=True) / tok.shape[1] + EPS)
        for pos in range(16):
            x1[pos] = (xf[pos] * scale * gain1[pl.ds(block_of(pos), 1), :]).astype(jnp.bfloat16)

    def gate_task(second, positions):
        gw, uw = (w3, w4) if second else (w0, w1)
        gates = values = None
        for pos in positions:
            if second:
                rows = x2[:, pos].astype(jnp.float32).reshape(tok.shape[0], wide).astype(jnp.bfloat16)
            else:
                rows = x1[pos]
            a, b = nt(rows, gw[pos]), nt(rows, uw[pos])
            gates, values = (a, b) if gates is None else (gates + a, values + b)
        if 0 in positions:
            acc[0], acc[1] = gates, values
        else:
            acc[0] += gates
            acc[1] += values

    def hidden_task():
        g = acc[0]
        hid[...] = (g / (1.0 + jnp.exp(-g)) * acc[1]).astype(jnp.bfloat16)

    def down_task(second, positions):
        for pos in positions:
            if second:
                term = 0.5 * jnp.dot(hid[...], w5[pos], preferred_element_type=jnp.float32)
            else:
                term = 0.5 * jnp.dot(hid[...], w2[pos, 0:hidden_rows], preferred_element_type=jnp.float32)
                term = term + jnp.dot(mix[...], w2[pos, hidden_rows : w2.shape[1]], preferred_element_type=jnp.float32)
            (t2 if second else t1)[:, pos] = term.reshape(ntp, share, wide).astype(jnp.bfloat16)

    def resid_task():
        collect(0, r1, 0, 16)
        rows = pl.ds(pl.multiple_of(tp * share, share), share)
        total = sum_terms(t1, r1, 0, 16)
        value = xf[:, rows, :] + total
        resid[...] = value
        squares = jnp.sum(jnp.sum(value * value, axis=0), axis=-1, keepdims=True)
        scale = lax.rsqrt(squares / tok.shape[1] + EPS)
        for pos in range(16):
            nrm[pos] = (resid[pos] * scale * gain2[pl.ds(block_of(pos), 1), :]).astype(jnp.bfloat16)
        x2[tp] = nrm[...]
        spread(1, lambda peer: nrm, x2, 0, 16)

    def finish_sum(i, lo, hi):
        collect(2 + i, r2, lo, hi)
        value = (resid[lo:hi] + sum_terms(t2, r2, lo, hi)).astype(jnp.bfloat16)
        fin[lo:hi] = value
        done[tp, lo:hi] = value
        spread(5 + i, lambda peer: fin.at[lo:hi], done, lo, hi)

    def finish_join(i, lo, hi):
        collect(5 + i, done, lo, hi)
        for pos in range(lo, hi):
            rows = done[:, pos].astype(jnp.float32).reshape(tok.shape[0], wide).astype(jnp.bfloat16)
            out[:, pl.ds(pl.multiple_of(block_of(pos) * wide, wide), wide)] = rows

    lag = 1 if PAIRED else 0
    state = {"g1": 0, "d1": 0, "g2": 0, "d2": 0, "rs": None, "ag": None, "x2": False, "group": 0}

    def ready(chains, key, t):
        steps = []
        while state[key] <= 8 and all(state[key] + (lag if state[key] else 0) <= t - OFFSETS[c] for c in chains):
            steps.append(state[key])
            state[key] += 1
        return steps

    def run_down(second, chains, key, t):
        positions = []
        for s in ready(chains, key, t):
            for c in chains:
                arrived(c, s)
            positions += steps_positions(s)
        if positions:
            down_task(second, positions)

    def tasks(t):
        if t == 0:
            norm_first()
        for s in ready((0, 1), "g1", t):
            arrived(0, s)
            arrived(1, s)
            gate_task(False, steps_positions(s))
            if s == 8:
                hidden_task()
        if state["g1"] == 9:
            run_down(False, (2,), "d1", t)
        if state["d1"] == 9 and state["rs"] is None:
            spread(0, lambda peer: t1.at[peer], r1, 0, 16)
            state["rs"] = t
        if state["rs"] is not None and state["ag"] is None and t >= state["rs"] + SUM_AFTER:
            resid_task()
            state["ag"] = t
        if state["ag"] is not None and t >= state["ag"] + JOIN_AFTER:
            if not state["x2"]:
                collect(1, x2, 0, 16)
                state["x2"] = True
            for s in ready((3, 4), "g2", t):
                arrived(3, s)
                arrived(4, s)
                gate_task(True, steps_positions(s))
                if s == 8:
                    hidden_task()
            if state["g2"] == 9:
                run_down(True, (5,), "d2", t)
        here = 1 + 2 * (state["d2"] - 1) if state["d2"] else 0
        here = 16 if state["d2"] == 9 else here
        while state["group"] < len(GROUPS) and GROUPS[state["group"]][1] <= here:
            i = state["group"]
            lo, hi = GROUPS[i]
            spread(2 + i, lambda peer: t2.at[peer, lo:hi], r2, lo, hi)
            state["group"] += 1

    for t in range(SLOTS + 12):
        for c in range(6):
            step = t - OFFSETS[c]
            if 0 <= step <= 8:
                hop(c, step)
        tasks(t)
    for i, (lo, hi) in enumerate(GROUPS):
        finish_sum(i, lo, hi)
    for i, (lo, hi) in enumerate(GROUPS):
        finish_join(i, lo, hi)
    for copy in sends:
        copy.wait_send()


def local(tok, mix, n1, g1, u1, d1, ow, n2, g2, u2, d2):
    ntp, nfs = lax.axis_size("tp"), lax.axis_size("fs")
    rows, width = tok.shape
    share, wide, hidden_rows, heads = rows // ntp, width // nfs, g1.shape[1], mix.shape[1]
    bf, f32 = jnp.bfloat16, jnp.float32
    vmem = pl.BlockSpec(memory_space=pltpu.VMEM)
    hbm = pl.BlockSpec(memory_space=pl.ANY)
    block = pltpu.VMEM((nfs, hidden_rows, wide), bf)
    per_peer = pltpu.VMEM((ntp, nfs, share, wide), bf)
    own = pltpu.VMEM((nfs, share, wide), bf)
    kinds = 2 + 2 * len(GROUPS)
    return pl.pallas_call(
        body,
        out_shape=jax.ShapeDtypeStruct((rows, width), bf),
        in_specs=[vmem, vmem, vmem, vmem, vmem, vmem, hbm, hbm, vmem, vmem, hbm],
        out_specs=vmem,
        scratch_shapes=[
            block, block, pltpu.VMEM((nfs, hidden_rows + heads, wide), bf), block, block, block,
            pltpu.VMEM((nfs, rows, wide), f32),
            pltpu.VMEM((nfs, rows, wide), bf),
            pltpu.VMEM((2, rows, hidden_rows), f32),
            pltpu.VMEM((rows, hidden_rows), bf),
            per_peer, per_peer, per_peer, per_peer, own, per_peer, own, per_peer,
            pltpu.VMEM((nfs, share, wide), f32),
            pltpu.SemaphoreType.DMA((3,)),
            pltpu.SemaphoreType.DMA((6, 2, 8)),
            pltpu.SemaphoreType.DMA((6, 2, 8)),
            pltpu.SemaphoreType.DMA((6, 16)),
            pltpu.SemaphoreType.DMA((6, 16)),
            pltpu.SemaphoreType.DMA((kinds, 16)),
            pltpu.SemaphoreType.DMA((kinds, 16)),
        ],
        compiler_params=pltpu.CompilerParams(
            collective_id=0, has_side_effects=True, vmem_limit_bytes=48 << 20
        ),
    )(tok, mix, n1.reshape(nfs, wide), n2.reshape(nfs, wide), g1, u1, d1, ow, g2, u2, d2)


def solution(mesh):
    in_specs = (
        P(("grp", "fs"), None),
        P(("grp", "fs"), "tp"),
        P(),
        P("fs", "tp"),
        P("fs", "tp"),
        P("tp", "fs"),
        P("tp", "fs"),
        P(),
        P("fs", "tp"),
        P("fs", "tp"),
        P("tp", "fs"),
    )
    out_specs = P(("grp", "fs"), None)
    return jax.shard_map(local, mesh=mesh, in_specs=in_specs, out_specs=out_specs, check_vma=False)
```

time: 400 us -> 181 us (0.45)
  waiting for transfers between devices: 220 us -> 0 us
  Pallas kernels: 0 us -> 175 us
  starting transfers between devices: 82 us -> 0 us
  blocking collectives: 63.3 us -> 0 us
  between operations: 13.6 us -> 0.13 us
  matrix products: 10.9 us -> 0 us
  other arithmetic: 4.25 us -> 0 us
    pallas_call x0 -> x1, Pallas kernels: none -> 175 us  [local(): pl.pallas_call(body, out_shape=jax.ShapeDtypeStruct((rows, width), bf), i...]
    all_gather x2 -> x0, waiting for transfers between devices: 135 us -> none  [side_by_side(): result, at, done = (lax.all_gather(both, axis, axis=dim, tiled=True), 0, [])]
    all_to_all x4 -> x0, waiting for transfers between devices: 84.4 us -> none  [the longest x3 68 us: sent_to_all(): lax.all_to_all(jnp.broadcast_to(array[None], (size, *array.shape)), axis,...]
    all_to_all x4 -> x0, starting transfers between devices: 81.8 us -> none  [the longest x3 66.1 us: sent_to_all(): lax.all_to_all(jnp.broadcast_to(array[None], (size, *array.shape)), axis,...]
    all_gather x2 -> x0, blocking collectives: 32 us -> none  [join_rows(): return lax.all_gather(row_block, 'tp', axis=0, tiled=True)]
    all_to_all x1 -> x0, blocking collectives: 31.3 us -> none  [sum_at_owner(): tiles = lax.all_to_all(in_blocks(array, dim, size), axis, 0, 0, tiled=True)]
    dot_general x5 -> x0, matrix products: 10.9 us -> none  [the longest x2 5.92 us: half_branch(): jnp.dot(hidden, gather_directly(down_weight, 'fs', 1), preferred_element_...]
    unnamed x22 -> x19, local copies, waits for them, and re-layouts: 0.95 us -> 5.72 us
  transfers between devices with their start and end apart: 6 -> 0, of which waited for: 4 -> 0; matrix products, arithmetic and copies ran while one was open for 3% -> 0% of each run, Pallas kernels for 0% -> 0%
where the time goes in v1:
time: 181 us
  Pallas kernels  175 us (97%)
  local copies, waits for them, and re-layouts  5.72 us (3%)
    pallas_call x1, Pallas kernels, local(): pl.pallas_call(body, out_shape=jax.ShapeDtypeStruct((rows, width), bf), i...  175 us
    unnamed x19, local copies, waits for them, and re-layouts  5.72 us

profile of v1, /device:TPU:65, one launch (start us, length us, event | category | flops | bytes accessed | tf_op | source)
XLA Modules:
  0.0 181.1 jit_solution(7915496209184640120)
XLA Ops:
  0.0 0.0 copy-start
  0.0 1.1 copy.12.g1
  1.1 1.0 copy.13.u1
  2.1 0.0 copy-start.3
  2.1 0.0 copy-start.6
  2.1 1.0 copy.14.g2
  3.1 0.0 copy-start.1
  3.1 0.0 copy-start.2
  3.1 0.0 copy-start.5
  3.2 1.1 copy.15.u2
  4.2 0.0 copy-done
  4.2 0.0 copy-done.3
  4.2 0.0 copy-done.6
  4.2 0.0 copy-done.1
  4.3 0.0 copy-done.2
  4.3 0.0 copy-done.5
  4.3 0.0 copy-start.4
  4.3 0.7 copy-done.4
  5.0 175.3 %shard_map.109 = bf16[128,2048]{1,0:T(8,128)(2,1)S(1)} custom-call(bf16[128,2048]{1,0:T(8,128)(2,1)S(1)} %copy-done, bf16[128,128]{1,0:T(8,128)(2,1)S(1)} %copy-done.3, f32[16,128]{1,0:T(8,128)S(1)} %bitcast.2, f32[16,128]{1,0:T(8,128)S(1)} %bitcast.3, bf16[128,352]{1,0:T(8,128)(2,1)S(1)} %copy.12.g1, bf16[128,352]{1,0:T(8,128)(2,1)S(1)} %copy.13.u1, ...), custom_call_target="tpu_custom_call" | custom-call | tf_op jit(solution)/shard_map/pallas_call | solution.py:312
  180.3 0.8 copy.17
Async XLA Ops:
  0.0 4.2 %copy-start = (bf16[128,2048]{1,0:T(8,128)(2,1)S(1)}, bf16[128,2048]{1,0:T(8,128)(2,1)}, u32[]{:S(2)}) copy-start(bf16[128,2048]{1,0:T(8,128)(2,1)} %tok.1) | copy-start | bytes 1572868
  2.1 2.1 %copy-start.3 = (bf16[128,128]{1,0:T(8,128)(2,1)S(1)}, bf16[128,128]{1,0:T(8,128)(2,1)}, u32[]{:S(2)}) copy-start(bf16[128,128]{1,0:T(8,128)(2,1)} %mix.1) | copy-start | bytes 98308
  2.1 2.1 %copy-start.6 = (f32[2048]{0:T(1024)S(1)}, f32[2048]{0:T(1024)}, u32[]{:S(2)}) copy-start(f32[2048]{0:T(1024)} %param.18) | copy-start | bytes 24580
  3.1 1.1 copy-start.1
  3.1 1.1 copy-start.2
  3.1 1.1 copy-start.5
  4.3 0.8 copy-start.4

commit v2 on v1

--- a/solution.py
+++ b/solution.py
@@ -8,11 +8,11 @@
 from jax.sharding import PartitionSpec as P
 
 EPS = 0.1
-PAIRED = False
+PAIRED = True
 RIGHT, LEFT = 0, 1
 FIRST, SECOND = (0, 1, 2), (3, 4, 5)
-OFFSETS = (0, 0, 1, 8, 8, 10)
-SLOTS = 19
+OFFSETS = (0, 0, 0, 6, 6, 6)
+SLOTS = 15
 SUM_AFTER = 3
 JOIN_AFTER = 3
 GROUPS = ((0, 9), (9, 13), (13, 16))
@@ -29,8 +29,9 @@
 
 
 def body(
-    tok, mix, gain1, gain2, g1, u1, d1, ow, g2, u2, d2,
+    tok_in, mix_in, gain1_in, gain2_in, g1, u1, d1, ow, g2, u2, d2,
     out,
+    tok, mix, gain1, gain2,
     w0, w1, w2, w3, w4, w5, xf, x1, acc, hid, t1, r1, t2, r2, nrm, x2, fin, done, resid,
     wsem, ssem, rsem, ysend, yrecv, xsend, xrecv,
 ):
@@ -42,7 +43,7 @@
     mate = gr + 1 - 2 * parity
     share = tok.shape[0] // ntp
     wide = tok.shape[1] // nz
-    hidden_rows = g1.shape[1]
+    hidden_rows = g1.shape[0]
 
     def block_of(pos):
         if pos == 0:
@@ -67,18 +68,14 @@
     if PAIRED:
         pl.semaphore_signal(barrier, device_id={"grp": mate}, device_id_type=pl.DeviceIdType.MESH)
 
-    loads = [
-        pltpu.make_async_copy(d1, w2.at[0, 0:hidden_rows], wsem.at[0]),
-        pltpu.make_async_copy(ow, w2.at[0, hidden_rows : w2.shape[1]], wsem.at[1]),
-        pltpu.make_async_copy(d2, w5.at[0], wsem.at[2]),
-    ]
+    sources = (
+        (g1, w0.at[0]), (u1, w1.at[0]), (d1, w2.at[0, 0:hidden_rows]), (ow, w2.at[0, hidden_rows : w2.shape[1]]),
+        (tok_in, tok), (gain1_in, gain1), (mix_in, mix), (gain2_in, gain2), (g2, w3.at[0]), (u2, w4.at[0]), (d2, w5.at[0]),
+    )
+    loads = [pltpu.make_async_copy(src, dst, wsem.at[i]) for i, (src, dst) in enumerate(sources)]
     for load in loads:
         load.start()
-    w0[0] = g1[...].T
-    w1[0] = u1[...].T
-    w3[0] = g2[...].T
-    w4[0] = u2[...].T
-    for load in loads:
+    for load in loads[:4]:
         load.wait()
     pl.semaphore_wait(barrier, 18 if PAIRED else 17)
 
@@ -249,6 +246,8 @@
 
     def tasks(t):
         if t == 0:
+            for load in loads[4:]:
+                load.wait()
             norm_first()
         for s in ready((0, 1), "g1", t):
             arrived(0, s)
@@ -304,7 +303,7 @@
     share, wide, hidden_rows, heads = rows // ntp, width // nfs, g1.shape[1], mix.shape[1]
     bf, f32 = jnp.bfloat16, jnp.float32
     vmem = pl.BlockSpec(memory_space=pltpu.VMEM)
-    hbm = pl.BlockSpec(memory_space=pl.ANY)
+    hbm = pl.BlockSpec(memory_space=pltpu.HBM)
     block = pltpu.VMEM((nfs, hidden_rows, wide), bf)
     per_peer = pltpu.VMEM((ntp, nfs, share, wide), bf)
     own = pltpu.VMEM((nfs, share, wide), bf)
@@ -312,9 +311,11 @@
     return pl.pallas_call(
         body,
         out_shape=jax.ShapeDtypeStruct((rows, width), bf),
-        in_specs=[vmem, vmem, vmem, vmem, vmem, vmem, hbm, hbm, vmem, vmem, hbm],
+        in_specs=[hbm] * 11,
         out_specs=vmem,
         scratch_shapes=[
+            pltpu.VMEM((rows, width), bf), pltpu.VMEM((rows, heads), bf),
+            pltpu.VMEM((nfs, wide), f32), pltpu.VMEM((nfs, wide), f32),
             block, block, pltpu.VMEM((nfs, hidden_rows + heads, wide), bf), block, block, block,
             pltpu.VMEM((nfs, rows, wide), f32),
             pltpu.VMEM((nfs, rows, wide), bf),
@@ -322,7 +323,7 @@
             pltpu.VMEM((rows, hidden_rows), bf),
             per_peer, per_peer, per_peer, per_peer, own, per_peer, own, per_peer,
             pltpu.VMEM((nfs, share, wide), f32),
-            pltpu.SemaphoreType.DMA((3,)),
+            pltpu.SemaphoreType.DMA((11,)),
             pltpu.SemaphoreType.DMA((6, 2, 8)),
             pltpu.SemaphoreType.DMA((6, 2, 8)),
             pltpu.SemaphoreType.DMA((6, 16)),
@@ -331,9 +332,9 @@
             pltpu.SemaphoreType.DMA((kinds, 16)),
         ],
         compiler_params=pltpu.CompilerParams(
-            collective_id=0, has_side_effects=True, vmem_limit_bytes=48 << 20
+            collective_id=0, has_side_effects=True, vmem_limit_bytes=67043328
         ),
-    )(tok, mix, n1.reshape(nfs, wide), n2.reshape(nfs, wide), g1, u1, d1, ow, g2, u2, d2)
+    )(tok, mix, n1.reshape(nfs, wide), n2.reshape(nfs, wide), g1.T, u1.T, d1, ow, g2.T, u2.T, d2)
 
 
 def solution(mesh):

time: 181 us -> 162 us (0.90)
  Pallas kernels: 175 us -> 160 us
  local copies, waits for them, and re-layouts: 5.72 us -> 1.88 us
    pallas_call x1, Pallas kernels: 175 us -> 160 us  [local(): pl.pallas_call(body, out_shape=jax.ShapeDtypeStruct((rows, width), bf), i...]
    unnamed x19 -> x1, local copies, waits for them, and re-layouts: 5.72 us -> 1.88 us
where the time goes in v2:
time: 162 us
  Pallas kernels  160 us (99%)
  local copies, waits for them, and re-layouts  1.88 us (1%)
    pallas_call x1, Pallas kernels, local(): pl.pallas_call(body, out_shape=jax.ShapeDtypeStruct((rows, width), bf), i...  160 us

profile of v2, /device:TPU:65, one launch (start us, length us, event | category | flops | bytes accessed | tf_op | source)
XLA Modules:
  0.0 162.2 jit_solution(16436853625293026875)
XLA Ops:
  0.0 160.3 %shard_map.109 = bf16[128,2048]{1,0:T(8,128)(2,1)} custom-call(bf16[128,2048]{1,0:T(8,128)(2,1)} %tok_in.1, bf16[128,128]{1,0:T(8,128)(2,1)} %mix_in.1, f32[16,128]{1,0:T(8,128)} %bitcast.10, f32[16,128]{1,0:T(8,128)} %bitcast.11, bf16[352,128]{1,0:T(8,128)(2,1)} %bitcast.6, bf16[352,128]{1,0:T(8,128)(2,1)} %bitcast.7, bf16[352,128]{1,0:T(8,128)(2,1)} %d1.1, ...), custom_call_target="tpu_custom_call" | custom-call | tf_op jit(solution)/shard_map/pallas_call | solution.py:311
  160.3 1.9 %copy.13 = bf16[128,2048]{1,0:T(8,128)(2,1)} copy(bf16[128,2048]{1,0:T(8,128)(2,1)} %shard_map.109) | data formatting | bytes 1048576

commit v3 on v2

v3 whole, which is shorter than its diff:
```python
import functools

import jax
import jax.numpy as jnp
from jax import lax
from jax.experimental import pallas as pl
from jax.experimental.pallas import tpu as pltpu
from jax.sharding import PartitionSpec as P

EPS = 0.1
PAIRED = True
RIGHT, LEFT = 0, 1
OFFSETS = (0, 0, 0, 6, 6, 6)
SUM_AFTER = 2
JOIN_AFTER = 2
GROUPS = ((0, 7), (7, 16))


def schedule(offsets=OFFSETS, sum_after=SUM_AFTER, join_after=JOIN_AFTER, groups=GROUPS, lag=1):
    events, at = [], {"g1": 0, "d1": 0, "g2": 0, "d2": 0}
    sent = joined = None
    summed, group, spare = None, 0, []

    def ready(chains, key, t):
        steps = []
        while at[key] <= 8 and all(at[key] + (lag if at[key] else 0) <= t - offsets[c] for c in chains):
            steps.append(at[key])
            at[key] += 1
        return steps

    for t in range(40):
        for c in range(6):
            if 0 <= t - offsets[c] <= 8:
                events.append(("hop", c, t - offsets[c]))
        if t == 0:
            events.append(("norm",))
        for step in ready((0, 1), "g1", t):
            events.append(("gate", 0, step))
            if step == 8:
                events.append(("hidden",))
        if at["g1"] == 9:
            for step in ready((2,), "d1", t):
                events.append(("down", 0, step))
        if at["d1"] == 9 and sent is None:
            events += [("pair", 0, 0, 16), ("spread", 0, 0, 16)]
            sent = t
        if sent is not None and summed is None and t >= sent + sum_after:
            events.append(("resid",))
            summed = t
        if summed is not None and t >= summed + join_after:
            if joined is None:
                events += [("forward", 1, 0, 16), ("join", 1, 0, 16)]
                joined = t
            for step in ready((3, 4), "g2", t):
                events.append(("gate", 1, step))
                if step == 8:
                    events.append(("hidden",))
            if at["g2"] == 9:
                for step in ready((5,), "d2", t):
                    events.append(("down", 1, step))
                    here = 16 if step == 8 else 2 * step + 1
                    while group < len(groups) and groups[group][1] <= here:
                        events.append(("pair", 2 + 2 * group) + groups[group])
                        group += 1
    for name, first in (("spread", 2), ("finish", 2), ("forward", 3), ("out", 3)):
        for i, (lo, hi) in enumerate(groups):
            events.append((name, first + 2 * i, lo, hi))
    return events


def steps_positions(step):
    if step == 0:
        return (0,)
    return (15,) if step == 8 else (2 * step - 1, 2 * step)


def nt(a, b):
    return lax.dot_general(a, b, (((1,), (1,)), ((), ())), preferred_element_type=jnp.float32)


def body(
    tok_in, mix_in, gain1_in, gain2_in, g1, u1, d1, ow, g2, u2, d2,
    out,
    tok, mix, gain1, gain2,
    w0, w1, w2, w3, w4, w5, xf, x1, acc, hid, t1, q1, s1, r1, t2, q2, s2, r2, nrm, x2, fin, done, resid,
    wsem, ssem, rsem, ysend, yrecv, xsend, xrecv,
):
    W = (w0, w1, w2, w3, w4, w5)
    z, tp, gr = lax.axis_index("fs"), lax.axis_index("tp"), lax.axis_index("grp")
    nz, ntp = lax.axis_size("fs"), lax.axis_size("tp")
    right, left = lax.rem(z + 1, nz), lax.rem(z + nz - 1, nz)
    parity = lax.rem(gr, 2)
    mate = gr + 1 - 2 * parity
    chips = ntp // 2
    chip, core = tp // 2, lax.rem(tp, 2)
    partner = tp + 1 - 2 * core
    share = tok.shape[0] // ntp
    wide = tok.shape[1] // nz
    hidden_rows = g1.shape[0]

    def block_of(pos):
        if pos == 0:
            return z
        if pos == 15:
            return lax.rem(z + 8, nz)
        step = (pos + 1) // 2
        return lax.rem(z + nz - step, nz) if pos % 2 else lax.rem(z + step, nz)

    def cut(c):
        rows = W[c].shape[1]
        lent = rows // 3 // 16 * 16
        if not PAIRED:
            return 0, rows, 0, 0
        return pl.multiple_of(parity * lent, 16), rows - lent, pl.multiple_of((1 - parity) * (rows - lent), 16), lent

    barrier = pltpu.get_barrier_semaphore()
    pl.semaphore_signal(barrier, device_id={"fs": right}, device_id_type=pl.DeviceIdType.MESH)
    pl.semaphore_signal(barrier, device_id={"fs": left}, device_id_type=pl.DeviceIdType.MESH)
    for d in range(1, chips):
        pl.semaphore_signal(barrier, device_id={"tp": lax.rem(tp + 2 * d, ntp)}, device_id_type=pl.DeviceIdType.MESH)
    pl.semaphore_signal(barrier, device_id={"tp": partner}, device_id_type=pl.DeviceIdType.MESH)
    if PAIRED:
        pl.semaphore_signal(barrier, device_id={"grp": mate}, device_id_type=pl.DeviceIdType.MESH)

    sources = (
        (g1, w0.at[0]), (u1, w1.at[0]), (d1, w2.at[0, 0:hidden_rows]), (ow, w2.at[0, hidden_rows : w2.shape[1]]),
        (tok_in, tok), (gain1_in, gain1), (mix_in, mix), (gain2_in, gain2), (g2, w3.at[0]), (u2, w4.at[0]), (d2, w5.at[0]),
    )
    loads = [pltpu.make_async_copy(src, dst, wsem.at[i]) for i, (src, dst) in enumerate(sources)]
    for load in loads:
        load.start()
    for load in loads[:4]:
        load.wait()
    pl.semaphore_wait(barrier, chips + (3 if PAIRED else 2))

    sends = []

    def start(copy):
        copy.start()
        sends.append(copy)

    def ring_copy(c, way, step):
        start, keep, _, _ = cut(c)
        if step == 7:
            half = keep // 32 * 16
            src = 13 if way == RIGHT else 14
            dst = 15
            rows = pl.ds(start, half) if way == RIGHT else pl.ds(start + half, keep - half)
        else:
            src = 0 if step == 0 else (2 * step - 1 if way == RIGHT else 2 * step)
            dst = 2 * step + 1 if way == RIGHT else 2 * step + 2
            rows = pl.ds(start, keep)
        return pltpu.make_async_remote_copy(
            src_ref=W[c].at[src, rows], dst_ref=W[c].at[dst, rows],
            send_sem=ssem.at[c, way, step], recv_sem=rsem.at[c, way, step],
            device_id={"fs": right if way == RIGHT else left}, device_id_type=pl.DeviceIdType.MESH,
        )

    def lend_copy(c, pos):
        _, _, start, lent = cut(c)
        start = pl.multiple_of((W[c].shape[1] - lent) - start, 16)
        return pltpu.make_async_remote_copy(
            src_ref=W[c].at[pos, pl.ds(start, lent)], dst_ref=W[c].at[pos, pl.ds(start, lent)],
            send_sem=ysend.at[c, pos], recv_sem=yrecv.at[c, pos],
            device_id={"grp": mate}, device_id_type=pl.DeviceIdType.MESH,
        )

    def hop(c, step):
        for way in (RIGHT, LEFT):
            if step > 0:
                ring_copy(c, way, step - 1).wait_recv()
            if step < 8:
                start(ring_copy(c, way, step))
            if PAIRED and 0 < step < 8:
                start(lend_copy(c, 2 * step - 1 if way == RIGHT else 2 * step))
        if PAIRED and step == 8:
            start(lend_copy(c, 15))

    def arrived(c, step):
        if PAIRED and step > 0:
            for pos in steps_positions(step):
                _, _, start, lent = cut(c)
                rows = pl.ds(start, lent)
                pltpu.make_async_remote_copy(
                    src_ref=W[c].at[pos, rows], dst_ref=W[c].at[pos, rows],
                    send_sem=ysend.at[c, pos], recv_sem=yrecv.at[c, pos],
                    device_id={"grp": mate}, device_id_type=pl.DeviceIdType.MESH,
                ).wait_recv()

    def to_peer(kind, i, src, dst, peer):
        return pltpu.make_async_remote_copy(
            src_ref=src, dst_ref=dst, send_sem=xsend.at[kind, i], recv_sem=xrecv.at[kind, i],
            device_id={"tp": peer}, device_id_type=pl.DeviceIdType.MESH,
        )

    def terms(kind):
        return (t1, q1, s1, r1) if kind == 0 else (t2, q2, s2, r2)

    def pair_send(kind, lo, hi):
        t, q, _, _ = terms(kind)
        start(to_peer(kind, 0, t.at[1 - core, :, lo:hi], q.at[:, lo:hi], partner))

    def spread(kind, lo, hi):
        t, q, s, r = terms(kind)
        to_peer(kind, 0, q.at[:, lo:hi], q.at[:, lo:hi], partner).wait_recv()
        s[:, lo:hi] = (t[core, :, lo:hi].astype(jnp.float32) + q[:, lo:hi].astype(jnp.float32)).astype(jnp.bfloat16)
        for d in range(1, chips):
            there = lax.rem(chip + d, chips)
            start(to_peer(kind, d, s.at[there, lo:hi], r.at[chip, lo:hi], lax.rem(tp + 2 * d, ntp)))

    def collect(kind, lo, hi):
        t, q, _, r = terms(kind)
        total = t[core, chip, lo:hi].astype(jnp.float32) + q[chip, lo:hi].astype(jnp.float32)
        for d in range(1, chips):
            part = r.at[lax.rem(chip + chips - d, chips), lo:hi]
            to_peer(kind, d, part, part, partner).wait_recv()
        for d in range(1, chips):
            total = total + r[lax.rem(chip + d, chips), lo:hi].astype(jnp.float32)
        return total

    def share_rows(kind, own, dst, lo, hi):
        for d in range(1, chips):
            start(to_peer(kind, d, own.at[lo:hi], dst.at[chip, core, lo:hi], lax.rem(tp + 2 * d, ntp)))
        start(to_peer(kind, 0, own.at[lo:hi], dst.at[chip, core, lo:hi], partner))

    def forward(kind, dst, lo, hi):
        for d in sorted(range(1, chips), key=lambda d: min(d, chips - d)):
            part = dst.at[lax.rem(chip + chips - d, chips), core, lo:hi]
            to_peer(kind, d, part, part, partner).wait_recv()
            start(to_peer(kind, chips + d, part, part, partner))

    def join(kind, dst, lo, hi):
        for d in range(chips):
            part = dst.at[lax.rem(chip + chips - d, chips), 1 - core, lo:hi]
            to_peer(kind, chips + d if d else 0, part, part, partner).wait_recv()

    def rows_of(ref, pos):
        return ref[:, :, pos].astype(jnp.float32).reshape(tok.shape[0], wide).astype(jnp.bfloat16)

    def norm_first():
        squares = jnp.zeros((tok.shape[0], wide), jnp.float32)
        for pos in range(16):
            b = block_of(pos)
            v = tok[:, pl.ds(pl.multiple_of(b * wide, wide), wide)].astype(jnp.float32)
            xf[pos] = v
            squares = squares + v * v
        scale = lax.rsqrt(jnp.sum(squares, axis=1, keepdims=True) / tok.shape[1] + EPS)
        for pos in range(16):
            x1[pos] = (xf[pos] * scale * gain1[pl.ds(block_of(pos), 1), :]).astype(jnp.bfloat16)

    def gate_task(second, positions):
        gw, uw = (w3, w4) if second else (w0, w1)
        gates = values = None
        for pos in positions:
            if second:
                rows = rows_of(x2, pos)
            else:
                rows = x1[pos]
            a, b = nt(rows, gw[pos]), nt(rows, uw[pos])
            gates, values = (a, b) if gates is None else (gates + a, values + b)
        if 0 in positions:
            acc[0], acc[1] = gates, values
        else:
            acc[0] += gates
            acc[1] += values

    def hidden_task():
        g = acc[0]
        hid[...] = (g / (1.0 + jnp.exp(-g)) * acc[1]).astype(jnp.bfloat16)

    def down_task(second, positions):
        for pos in positions:
            if second:
                term = 0.5 * jnp.dot(hid[...], w5[pos], preferred_element_type=jnp.float32)
            else:
                term = 0.5 * jnp.dot(hid[...], w2[pos, 0:hidden_rows], preferred_element_type=jnp.float32)
                term = term + jnp.dot(mix[...], w2[pos, hidden_rows : w2.shape[1]], preferred_element_type=jnp.float32)
            term = term.reshape(chips, 2, share, wide).astype(jnp.bfloat16)
            for c in range(2):
                (t2 if second else t1)[c, :, pos] = term[:, c]

    def resid_task():
        total = collect(0, 0, 16)
        rows = pl.ds(pl.multiple_of(tp * share, share), share)
        value = xf[:, rows, :] + total
        resid[...] = value
        squares = jnp.sum(jnp.sum(value * value, axis=0), axis=-1, keepdims=True)
        scale = lax.rsqrt(squares / tok.shape[1] + EPS)
        for pos in range(16):
            nrm[pos] = (resid[pos] * scale * gain2[pl.ds(block_of(pos), 1), :]).astype(jnp.bfloat16)
        share_rows(1, nrm, x2, 0, 16)
        x2[chip, core] = nrm[...]

    for event in schedule(lag=1 if PAIRED else 0):
        name, args = event[0], event[1:]
        if name == "hop":
            if args == (3, 0):
                for load in loads[8:]:
                    load.wait()
            hop(*args)
        elif name == "norm":
            for load in loads[4:8]:
                load.wait()
            norm_first()
        elif name == "gate":
            second, step = args
            for c in (3, 4) if second else (0, 1):
                arrived(c, step)
            gate_task(second, steps_positions(step))
        elif name == "hidden":
            hidden_task()
        elif name == "down":
            second, step = args
            arrived(5 if second else 2, step)
            down_task(second, steps_positions(step))
        elif name == "pair":
            pair_send(*args)
        elif name == "spread":
            spread(*args)
        elif name == "resid":
            resid_task()
        elif name == "finish":
            kind, lo, hi = args
            fin[lo:hi] = (resid[lo:hi] + collect(kind, lo, hi)).astype(jnp.bfloat16)
            share_rows(kind + 1, fin, done, lo, hi)
            done[chip, core, lo:hi] = fin[lo:hi]
        elif name == "forward":
            forward(args[0], x2 if args[0] == 1 else done, *args[1:])
        elif name == "join":
            join(args[0], x2, *args[1:])
        elif name == "out":
            kind, lo, hi = args
            join(kind, done, lo, hi)
            for pos in range(lo, hi):
                out[:, pl.ds(pl.multiple_of(block_of(pos) * wide, wide), wide)] = rows_of(done, pos)
    for copy in sends:
        copy.wait_send()


def local(tok, mix, n1, g1, u1, d1, ow, n2, g2, u2, d2):
    ntp, nfs = lax.axis_size("tp"), lax.axis_size("fs")
    rows, width = tok.shape
    share, wide, hidden_rows, heads = rows // ntp, width // nfs, g1.shape[1], mix.shape[1]
    chips = ntp // 2
    bf, f32 = jnp.bfloat16, jnp.float32
    vmem = pl.BlockSpec(memory_space=pltpu.VMEM)
    hbm = pl.BlockSpec(memory_space=pltpu.HBM)
    block = pltpu.VMEM((nfs, hidden_rows, wide), bf)
    both = pltpu.VMEM((2, chips, nfs, share, wide), bf)
    joined = pltpu.VMEM((chips, 2, nfs, share, wide), bf)
    half = pltpu.VMEM((chips, nfs, share, wide), bf)
    own = pltpu.VMEM((nfs, share, wide), bf)
    kinds = 2 + 2 * len(GROUPS)
    return pl.pallas_call(
        body,
        out_shape=jax.ShapeDtypeStruct((rows, width), bf),
        in_specs=[hbm] * 11,
        out_specs=vmem,
        scratch_shapes=[
            pltpu.VMEM((rows, width), bf), pltpu.VMEM((rows, heads), bf),
            pltpu.VMEM((nfs, wide), f32), pltpu.VMEM((nfs, wide), f32),
            block, block, pltpu.VMEM((nfs, hidden_rows + heads, wide), bf), block, block, block,
            pltpu.VMEM((nfs, rows, wide), f32),
            pltpu.VMEM((nfs, rows, wide), bf),
            pltpu.VMEM((2, rows, hidden_rows), f32),
            pltpu.VMEM((rows, hidden_rows), bf),
            both, half, half, half, both, half, half, half, own, joined, own, joined,
            pltpu.VMEM((nfs, share, wide), f32),
            pltpu.SemaphoreType.DMA((11,)),
            pltpu.SemaphoreType.DMA((6, 2, 8)),
            pltpu.SemaphoreType.DMA((6, 2, 8)),
            pltpu.SemaphoreType.DMA((6, 16)),
            pltpu.SemaphoreType.DMA((6, 16)),
            pltpu.SemaphoreType.DMA((kinds, 16)),
            pltpu.SemaphoreType.DMA((kinds, 16)),
        ],
        compiler_params=pltpu.CompilerParams(
            collective_id=0, has_side_effects=True, vmem_limit_bytes=67043328
        ),
    )(tok, mix, n1.reshape(nfs, wide), n2.reshape(nfs, wide), g1.T, u1.T, d1, ow, g2.T, u2.T, d2)


def solution(mesh):
    in_specs = (
        P(("grp", "fs"), None),
        P(("grp", "fs"), "tp"),
        P(),
        P("fs", "tp"),
        P("fs", "tp"),
        P("tp", "fs"),
        P("tp", "fs"),
        P(),
        P("fs", "tp"),
        P("fs", "tp"),
        P("tp", "fs"),
    )
    out_specs = P(("grp", "fs"), None)
    return jax.shard_map(local, mesh=mesh, in_specs=in_specs, out_specs=out_specs, check_vma=False)
```

time: 162 us -> 151 us (0.932)
  Pallas kernels: 160 us -> 149 us
    pallas_call x1, Pallas kernels: 160 us -> 149 us  [local(): pl.pallas_call(body, out_shape=jax.ShapeDtypeStruct((rows, width), bf), i...]
where the time goes in v3:
time: 151 us; the launch traced here: 150 us
  Pallas kernels  149 us (99%)
  local copies, waits for them, and re-layouts  1.88 us (1%)
    pallas_call x1, Pallas kernels, local(): pl.pallas_call(body, out_shape=jax.ShapeDtypeStruct((rows, width), bf), i...  149 us

profile of v3, /device:TPU:65, one launch (start us, length us, event | category | flops | bytes accessed | tf_op | source)
XLA Modules:
  0.0 150.5 jit_solution(2674889160007070443)
XLA Ops:
  0.0 148.6 %shard_map.109 = bf16[128,2048]{1,0:T(8,128)(2,1)} custom-call(bf16[128,2048]{1,0:T(8,128)(2,1)} %tok_in.1, bf16[128,128]{1,0:T(8,128)(2,1)} %mix_in.1, f32[16,128]{1,0:T(8,128)} %bitcast.10, f32[16,128]{1,0:T(8,128)} %bitcast.11, bf16[352,128]{1,0:T(8,128)(2,1)} %bitcast.6, bf16[352,128]{1,0:T(8,128)(2,1)} %bitcast.7, bf16[352,128]{1,0:T(8,128)(2,1)} %d1.1, ...), custom_call_target="tpu_custom_call" | custom-call | tf_op jit(solution)/shard_map/pallas_call | solution.py:354
  148.6 1.9 %copy.13 = bf16[128,2048]{1,0:T(8,128)(2,1)} copy(bf16[128,2048]{1,0:T(8,128)(2,1)} %shard_map.109) | data formatting | bytes 1048576

commit v4 on v3

--- a/solution.py
+++ b/solution.py
@@ -10,62 +10,37 @@
 EPS = 0.1
 PAIRED = True
 RIGHT, LEFT = 0, 1
-OFFSETS = (0, 0, 0, 6, 6, 6)
-SUM_AFTER = 2
-JOIN_AFTER = 2
-GROUPS = ((0, 7), (7, 16))
-
-
-def schedule(offsets=OFFSETS, sum_after=SUM_AFTER, join_after=JOIN_AFTER, groups=GROUPS, lag=1):
-    events, at = [], {"g1": 0, "d1": 0, "g2": 0, "d2": 0}
-    sent = joined = None
-    summed, group, spare = None, 0, []
-
-    def ready(chains, key, t):
-        steps = []
-        while at[key] <= 8 and all(at[key] + (lag if at[key] else 0) <= t - offsets[c] for c in chains):
-            steps.append(at[key])
-            at[key] += 1
-        return steps
-
-    for t in range(40):
-        for c in range(6):
-            if 0 <= t - offsets[c] <= 8:
-                events.append(("hop", c, t - offsets[c]))
-        if t == 0:
-            events.append(("norm",))
-        for step in ready((0, 1), "g1", t):
-            events.append(("gate", 0, step))
-            if step == 8:
-                events.append(("hidden",))
-        if at["g1"] == 9:
-            for step in ready((2,), "d1", t):
-                events.append(("down", 0, step))
-        if at["d1"] == 9 and sent is None:
-            events += [("pair", 0, 0, 16), ("spread", 0, 0, 16)]
-            sent = t
-        if sent is not None and summed is None and t >= sent + sum_after:
-            events.append(("resid",))
-            summed = t
-        if summed is not None and t >= summed + join_after:
-            if joined is None:
-                events += [("forward", 1, 0, 16), ("join", 1, 0, 16)]
-                joined = t
-            for step in ready((3, 4), "g2", t):
-                events.append(("gate", 1, step))
-                if step == 8:
-                    events.append(("hidden",))
-            if at["g2"] == 9:
-                for step in ready((5,), "d2", t):
-                    events.append(("down", 1, step))
-                    here = 16 if step == 8 else 2 * step + 1
-                    while group < len(groups) and groups[group][1] <= here:
-                        events.append(("pair", 2 + 2 * group) + groups[group])
-                        group += 1
-    for name, first in (("spread", 2), ("finish", 2), ("forward", 3), ("out", 3)):
-        for i, (lo, hi) in enumerate(groups):
-            events.append((name, first + 2 * i, lo, hi))
-    return events
+SCALES = 2
+EVENTS = (
+    ("hop", 0, 0, 0), ("hop", 0, 0, 1), ("hop", 1, 0, 0), ("hop", 1, 0, 1), ("hop", 2, 0, 0), ("hop", 2, 0, 1),
+    ("hop", 0, 1, 0), ("hop", 0, 1, 1), ("hop", 1, 1, 0), ("hop", 1, 1, 1), ("hop", 2, 1, 0), ("hop", 2, 1, 1),
+    ("hop", 0, 2, 0), ("hop", 0, 2, 1), ("hop", 1, 2, 0), ("hop", 1, 2, 1), ("norm",), ("hop", 2, 2, 0),
+    ("hop", 2, 2, 1), ("hop", 0, 3, 0), ("hop", 0, 3, 1), ("hop", 1, 3, 0), ("hop", 1, 3, 1), ("hop", 2, 3, 0),
+    ("gate", 0, 0), ("hop", 2, 3, 1), ("hop", 0, 4, 0), ("hop", 0, 4, 1), ("hop", 1, 4, 0), ("hop", 1, 4, 1),
+    ("hop", 2, 4, 0), ("hop", 2, 4, 1), ("hop", 0, 5, 0), ("hop", 0, 5, 1), ("hop", 1, 5, 0), ("hop", 1, 5, 1),
+    ("hop", 2, 5, 0), ("hop", 2, 5, 1), ("hop", 0, 6, 0), ("hop", 0, 6, 1), ("hop", 1, 6, 0), ("hop", 1, 6, 1),
+    ("gate", 0, 5), ("hop", 2, 6, 0), ("hop", 2, 6, 1), ("gate", 0, 1), ("hop", 3, 0, 0), ("hop", 3, 0, 1),
+    ("hop", 4, 0, 0), ("hop", 4, 0, 1), ("hop", 0, 7, 0), ("hop", 0, 7, 1), ("hop", 1, 7, 0), ("hop", 1, 7, 1),
+    ("gate", 0, 6), ("hop", 2, 7, 0), ("hop", 2, 7, 1), ("hop", 3, 1, 0), ("hop", 3, 1, 1), ("gate", 0, 2),
+    ("hop", 4, 1, 0), ("gate", 0, 4), ("hop", 4, 1, 1), ("hop", 5, 0, 0), ("gate", 0, 3), ("hop", 5, 0, 1),
+    ("hop", 0, 8, 0), ("hop", 0, 8, 1), ("hop", 1, 8, 0), ("hop", 1, 8, 1), ("hop", 2, 8, 0), ("hop", 2, 8, 1),
+    ("hop", 3, 2, 0), ("hop", 3, 2, 1), ("hop", 4, 2, 0), ("gate", 0, 7), ("hop", 4, 2, 1), ("gate", 0, 8),
+    ("hidden", 0), ("down", 0, 5), ("hop", 5, 1, 0), ("hop", 5, 1, 1), ("down", 0, 2), ("down", 0, 3),
+    ("down", 0, 1), ("down", 0, 8), ("hop", 3, 3, 0), ("down", 0, 4), ("hop", 3, 3, 1), ("down", 0, 0),
+    ("down", 0, 7), ("down", 0, 6), ("hop", 4, 3, 0), ("hop", 4, 3, 1), ("pair", 0, 0, 16), ("hop", 5, 2, 0),
+    ("hop", 5, 2, 1), ("spread", 0, 0, 16), ("hop", 3, 4, 0), ("hop", 3, 4, 1), ("hop", 4, 4, 0), ("hop", 4, 4, 1),
+    ("hop", 5, 3, 0), ("hop", 5, 3, 1), ("hop", 3, 5, 0), ("hop", 3, 5, 1), ("hop", 4, 5, 0), ("hop", 4, 5, 1),
+    ("hop", 5, 4, 0), ("hop", 5, 4, 1), ("collect", 0, 0, 16), ("hop", 3, 6, 0), ("hop", 3, 6, 1), ("hop", 4, 6, 0),
+    ("hop", 4, 6, 1), ("hop", 5, 5, 0), ("hop", 5, 5, 1), ("scale", 2), ("hop", 3, 7, 0), ("hop", 3, 7, 1),
+    ("hop", 4, 7, 0), ("hop", 4, 7, 1), ("forward", 1, 0, 16), ("hop", 5, 6, 0), ("hop", 5, 6, 1), ("hop", 3, 8, 0),
+    ("join", 1, 0, 16), ("gate", 1, 0), ("hop", 3, 8, 1), ("forward", 2, 0, 1), ("gate", 1, 1), ("hop", 4, 8, 0),
+    ("hop", 4, 8, 1), ("gate", 1, 7), ("gate", 1, 6), ("gate", 1, 2), ("hop", 5, 7, 0), ("hop", 5, 7, 1),
+    ("gate", 1, 5), ("gate", 1, 3), ("gate", 1, 8), ("gate", 1, 4), ("join", 2, 0, 1), ("hidden", 1), ("down", 1, 1),
+    ("hop", 5, 8, 0), ("hop", 5, 8, 1), ("down", 1, 3), ("down", 1, 4), ("down", 1, 6), ("down", 1, 5),
+    ("down", 1, 0), ("down", 1, 7), ("down", 1, 2), ("pair", 3, 0, 9), ("down", 1, 8), ("pair", 5, 9, 16),
+    ("spread", 3, 0, 9), ("spread", 5, 9, 16), ("finish", 3, 0, 9), ("finish", 5, 9, 16), ("forward", 4, 0, 9),
+    ("forward", 6, 9, 16), ("out", 4, 0, 9), ("out", 6, 9, 16),
+)
 
 
 def steps_positions(step):
@@ -82,7 +57,7 @@
     tok_in, mix_in, gain1_in, gain2_in, g1, u1, d1, ow, g2, u2, d2,
     out,
     tok, mix, gain1, gain2,
-    w0, w1, w2, w3, w4, w5, xf, x1, acc, hid, t1, q1, s1, r1, t2, q2, s2, r2, nrm, x2, fin, done, resid,
+    w0, w1, w2, w3, w4, w5, xf, x1, acc, hid, t1, q1, s1, r1, t2, q2, s2, r2, nrm, x2, fin, done, resid, squares, mine, scales,
     wsem, ssem, rsem, ysend, yrecv, xsend, xrecv,
 ):
     W = (w0, w1, w2, w3, w4, w5)
@@ -129,8 +104,6 @@
     loads = [pltpu.make_async_copy(src, dst, wsem.at[i]) for i, (src, dst) in enumerate(sources)]
     for load in loads:
         load.start()
-    for load in loads[:4]:
-        load.wait()
     pl.semaphore_wait(barrier, chips + (3 if PAIRED else 2))
 
     sends = []
@@ -165,15 +138,14 @@
             device_id={"grp": mate}, device_id_type=pl.DeviceIdType.MESH,
         )
 
-    def hop(c, step):
-        for way in (RIGHT, LEFT):
-            if step > 0:
-                ring_copy(c, way, step - 1).wait_recv()
-            if step < 8:
-                start(ring_copy(c, way, step))
-            if PAIRED and 0 < step < 8:
-                start(lend_copy(c, 2 * step - 1 if way == RIGHT else 2 * step))
-        if PAIRED and step == 8:
+    def hop(c, step, way):
+        if step > 0:
+            ring_copy(c, way, step - 1).wait_recv()
+        if step < 8:
+            start(ring_copy(c, way, step))
+        if PAIRED and 0 < step < 8:
+            start(lend_copy(c, 2 * step - 1 if way == RIGHT else 2 * step))
+        if PAIRED and step == 8 and way == LEFT:
             start(lend_copy(c, 15))
 
     def arrived(c, step):
@@ -193,8 +165,10 @@
             device_id={"tp": peer}, device_id_type=pl.DeviceIdType.MESH,
         )
 
+    far_first = sorted(range(1, chips), key=lambda d: -min(d, chips - d))
+
     def terms(kind):
-        return (t1, q1, s1, r1) if kind == 0 else (t2, q2, s2, r2)
+        return (t1, q1, s1, r1) if kind < SCALES else (t2, q2, s2, r2)
 
     def pair_send(kind, lo, hi):
         t, q, _, _ = terms(kind)
@@ -204,7 +178,7 @@
         t, q, s, r = terms(kind)
         to_peer(kind, 0, q.at[:, lo:hi], q.at[:, lo:hi], partner).wait_recv()
         s[:, lo:hi] = (t[core, :, lo:hi].astype(jnp.float32) + q[:, lo:hi].astype(jnp.float32)).astype(jnp.bfloat16)
-        for d in range(1, chips):
+        for d in far_first:
             there = lax.rem(chip + d, chips)
             start(to_peer(kind, d, s.at[there, lo:hi], r.at[chip, lo:hi], lax.rem(tp + 2 * d, ntp)))
 
@@ -219,12 +193,12 @@
         return total
 
     def share_rows(kind, own, dst, lo, hi):
-        for d in range(1, chips):
+        for d in far_first:
             start(to_peer(kind, d, own.at[lo:hi], dst.at[chip, core, lo:hi], lax.rem(tp + 2 * d, ntp)))
         start(to_peer(kind, 0, own.at[lo:hi], dst.at[chip, core, lo:hi], partner))
 
     def forward(kind, dst, lo, hi):
-        for d in sorted(range(1, chips), key=lambda d: min(d, chips - d)):
+        for d in far_first:
             part = dst.at[lax.rem(chip + chips - d, chips), core, lo:hi]
             to_peer(kind, d, part, part, partner).wait_recv()
             start(to_peer(kind, chips + d, part, part, partner))
@@ -264,9 +238,12 @@
             acc[0] += gates
             acc[1] += values
 
-    def hidden_task():
-        g = acc[0]
-        hid[...] = (g / (1.0 + jnp.exp(-g)) * acc[1]).astype(jnp.bfloat16)
+    def hidden_task(second):
+        g, v = acc[0], acc[1]
+        if second:
+            scale = scales[:, :, 0].reshape(tok.shape[0], wide)[:, 0:1]
+            g, v = g * scale, v * scale
+        hid[...] = (g / (1.0 + jnp.exp(-g)) * v).astype(jnp.bfloat16)
 
     def down_task(second, positions):
         for pos in positions:
@@ -279,60 +256,79 @@
             for c in range(2):
                 (t2 if second else t1)[c, :, pos] = term[:, c]
 
-    def resid_task():
-        total = collect(0, 0, 16)
+    def collect_task(kind, lo, hi):
         rows = pl.ds(pl.multiple_of(tp * share, share), share)
-        value = xf[:, rows, :] + total
-        resid[...] = value
-        squares = jnp.sum(jnp.sum(value * value, axis=0), axis=-1, keepdims=True)
-        scale = lax.rsqrt(squares / tok.shape[1] + EPS)
-        for pos in range(16):
-            nrm[pos] = (resid[pos] * scale * gain2[pl.ds(block_of(pos), 1), :]).astype(jnp.bfloat16)
-        share_rows(1, nrm, x2, 0, 16)
-        x2[chip, core] = nrm[...]
-
-    for event in schedule(lag=1 if PAIRED else 0):
-        name, args = event[0], event[1:]
+        value = xf[lo:hi, rows, :] + collect(kind, lo, hi)
+        resid[lo:hi] = value
+        here = jnp.sum(value * value, axis=0)
+        squares[...] = here if kind == 0 else squares[...] + here
+        for pos in range(lo, hi):
+            nrm[pos] = (resid[pos] * gain2[pl.ds(block_of(pos), 1), :]).astype(jnp.bfloat16)
+        x2[chip, core, lo:hi] = nrm[lo:hi]
+        share_rows(kind + 1, nrm, x2, lo, hi)
+
+    def scale_task(kind):
+        total = jnp.sum(squares[...], axis=-1, keepdims=True)
+        scale = jnp.broadcast_to(lax.rsqrt(total / tok.shape[1] + EPS), squares.shape)
+        mine[0] = scale
+        scales[chip, core, 0] = scale
+        share_rows(kind, mine, scales, 0, 1)
+
+    def landing(kind):
+        return x2 if kind < SCALES else (scales if kind == SCALES else done)
+
+    def finish_task(kind, lo, hi):
+        fin[lo:hi] = (resid[lo:hi] + collect(kind, lo, hi)).astype(jnp.bfloat16)
+        share_rows(kind + 1, fin, done, lo, hi)
+        done[chip, core, lo:hi] = fin[lo:hi]
+
+    def out_task(kind, lo, hi):
+        join(kind, done, lo, hi)
+        for pos in range(lo, hi):
+            out[:, pl.ds(pl.multiple_of(block_of(pos) * wide, wide), wide)] = rows_of(done, pos)
+
+    waited = set()
+
+    def need(*numbers):
+        for i in numbers:
+            if i not in waited:
+                loads[i].wait()
+                waited.add(i)
+
+    own_loads = ((0,), (1,), (2, 3), (8,), (9,), (10,))
+    for name, *args in EVENTS:
         if name == "hop":
-            if args == (3, 0):
-                for load in loads[8:]:
-                    load.wait()
+            if args[1] == 0:
+                need(*own_loads[args[0]])
             hop(*args)
         elif name == "norm":
-            for load in loads[4:8]:
-                load.wait()
+            need(4, 5, 6, 7)
             norm_first()
         elif name == "gate":
-            second, step = args
-            for c in (3, 4) if second else (0, 1):
-                arrived(c, step)
-            gate_task(second, steps_positions(step))
+            for c in (3, 4) if args[0] else (0, 1):
+                arrived(c, args[1])
+            gate_task(args[0], steps_positions(args[1]))
         elif name == "hidden":
-            hidden_task()
+            hidden_task(args[0])
         elif name == "down":
-            second, step = args
-            arrived(5 if second else 2, step)
-            down_task(second, steps_positions(step))
+            arrived(5 if args[0] else 2, args[1])
+            down_task(args[0], steps_positions(args[1]))
         elif name == "pair":
             pair_send(*args)
         elif name == "spread":
             spread(*args)
-        elif name == "resid":
-            resid_task()
+        elif name == "collect":
+            collect_task(*args)
+        elif name == "scale":
+            scale_task(*args)
+        elif name == "forward":
+            forward(args[0], landing(args[0]), *args[1:])
+        elif name == "join":
+            join(args[0], landing(args[0]), *args[1:])
         elif name == "finish":
-            kind, lo, hi = args
-            fin[lo:hi] = (resid[lo:hi] + collect(kind, lo, hi)).astype(jnp.bfloat16)
-            share_rows(kind + 1, fin, done, lo, hi)
-            done[chip, core, lo:hi] = fin[lo:hi]
-        elif name == "forward":
-            forward(args[0], x2 if args[0] == 1 else done, *args[1:])
-        elif name == "join":
-            join(args[0], x2, *args[1:])
-        elif name == "out":
-            kind, lo, hi = args
-            join(kind, done, lo, hi)
-            for pos in range(lo, hi):
-                out[:, pl.ds(pl.multiple_of(block_of(pos) * wide, wide), wide)] = rows_of(done, pos)
+            finish_task(*args)
+        else:
+            out_task(*args)
     for copy in sends:
         copy.wait_send()
 
@@ -350,7 +346,7 @@
     joined = pltpu.VMEM((chips, 2, nfs, share, wide), bf)
     half = pltpu.VMEM((chips, nfs, share, wide), bf)
     own = pltpu.VMEM((nfs, share, wide), bf)
-    kinds = 2 + 2 * len(GROUPS)
+    kinds = 1 + max(event[1] for event in EVENTS if event[0] == "out")
     return pl.pallas_call(
         body,
         out_shape=jax.ShapeDtypeStruct((rows, width), bf),
@@ -365,7 +361,8 @@
             pltpu.VMEM((2, rows, hidden_rows), f32),
             pltpu.VMEM((rows, hidden_rows), bf),
             both, half, half, half, both, half, half, half, own, joined, own, joined,
-            pltpu.VMEM((nfs, share, wide), f32),
+            pltpu.VMEM((nfs, share, wide), f32), pltpu.VMEM((share, wide), f32),
+            pltpu.VMEM((1, share, wide), f32), pltpu.VMEM((chips, 2, 1, share, wide), f32),
             pltpu.SemaphoreType.DMA((11,)),
             pltpu.SemaphoreType.DMA((6, 2, 8)),
             pltpu.SemaphoreType.DMA((6, 2, 8)),

time: 151 us -> 147 us (0.974)
  Pallas kernels: 149 us -> 145 us
    pallas_call x1, Pallas kernels: 149 us -> 145 us  [local(): pl.pallas_call(body, out_shape=jax.ShapeDtypeStruct((rows, width), bf), i...]
where the time goes in v4:
time: 147 us
  Pallas kernels  145 us (99%)
  local copies, waits for them, and re-layouts  1.88 us (1%)
    pallas_call x1, Pallas kernels, local(): pl.pallas_call(body, out_shape=jax.ShapeDtypeStruct((rows, width), bf), i...  145 us

profile of v4, /device:TPU:65, one launch (start us, length us, event | category | flops | bytes accessed | tf_op | source)
XLA Modules:
  0.0 146.6 jit_solution(11393765805187388192)
XLA Ops:
  0.0 144.7 %shard_map.109 = bf16[128,2048]{1,0:T(8,128)(2,1)} custom-call(bf16[128,2048]{1,0:T(8,128)(2,1)} %tok_in.1, bf16[128,128]{1,0:T(8,128)(2,1)} %mix_in.1, f32[16,128]{1,0:T(8,128)} %bitcast.10, f32[16,128]{1,0:T(8,128)} %bitcast.11, bf16[352,128]{1,0:T(8,128)(2,1)} %bitcast.6, bf16[352,128]{1,0:T(8,128)(2,1)} %bitcast.7, bf16[352,128]{1,0:T(8,128)(2,1)} %d1.1, ...), custom_call_target="tpu_custom_call" | custom-call | tf_op jit(solution)/shard_map/pallas_call | solution.py:350
  144.7 1.9 %copy.13 = bf16[128,2048]{1,0:T(8,128)(2,1)} copy(bf16[128,2048]{1,0:T(8,128)(2,1)} %shard_map.109) | data formatting | bytes 1048576

commit v5 on v4

--- a/solution.py
+++ b/solution.py
@@ -83,7 +83,7 @@
 
     def cut(c):
         rows = W[c].shape[1]
-        lent = rows // 3 // 16 * 16
+        lent = (rows - 1) // 3 // 16 * 16
         if not PAIRED:
             return 0, rows, 0, 0
         return pl.multiple_of(parity * lent, 16), rows - lent, pl.multiple_of((1 - parity) * (rows - lent), 16), lent

time: 147 us -> 147 us (level)
  no operation moved by 1% of the time
where the time goes in v5:
time: 147 us
  Pallas kernels  145 us (99%)
  local copies, waits for them, and re-layouts  1.88 us (1%)
    pallas_call x1, Pallas kernels, local(): pl.pallas_call(body, out_shape=jax.ShapeDtypeStruct((rows, width), bf), i...  145 us

profile of v5, /device:TPU:65, one launch (start us, length us, event | category | flops | bytes accessed | tf_op | source)
XLA Modules:
  0.0 147.2 jit_solution(7327598165729674581)
XLA Ops:
  0.0 145.3 %shard_map.109 = bf16[128,2048]{1,0:T(8,128)(2,1)} custom-call(bf16[128,2048]{1,0:T(8,128)(2,1)} %tok_in.1, bf16[128,128]{1,0:T(8,128)(2,1)} %mix_in.1, f32[16,128]{1,0:T(8,128)} %bitcast.10, f32[16,128]{1,0:T(8,128)} %bitcast.11, bf16[352,128]{1,0:T(8,128)(2,1)} %bitcast.6, bf16[352,128]{1,0:T(8,128)(2,1)} %bitcast.7, bf16[352,128]{1,0:T(8,128)(2,1)} %d1.1, ...), custom_call_target="tpu_custom_call" | custom-call | tf_op jit(solution)/shard_map/pallas_call | solution.py:350
  145.4 1.9 %copy.13 = bf16[128,2048]{1,0:T(8,128)(2,1)} copy(bf16[128,2048]{1,0:T(8,128)(2,1)} %shard_map.109) | data formatting | bytes 1048576
